TPU v7x, 256 devices: a whole 4x4x8 slice. The times are simulated.
256 devices in a mesh: fs: 32 (over z, x), tp: 8 (over y, core).
Axes of the slice: x: 4, y: 4, z: 8, core: 2. Of those that a mesh axis runs over, the one named last changes fastest.
Arguments:
- tokens: bfloat16 [1280, 4096], P('fs'), may hold values from -6 to 6
- routes: int32 [1280, 2], P('fs'), may hold values from 0 to 3, all different within a row; in each aligned block of 40 rows (0 to 39, 40 to 79, ...) at most 30 rows name the same one
- route_logits: float32 [1280, 2], P('fs'), may hold values from -6 to 6
- norm_gain: float32 [4096], P('fs'), may hold values from 0.1 to 1.9
- gate_weight: float32 [4, 4096, 8192], P(None, 'fs', 'tp'), may hold values from -0.09375 to 0.09375
- up_weight: float32 [4, 4096, 8192], P(None, 'fs', 'tp'), may hold values from -0.09375 to 0.09375
- down_weight: float32 [4, 4096, 8192], P(None, 'fs', 'tp'), may hold values from -0.0625 to 0.0625
Outputs:
- mixed: bfloat16 [1280, 4096], P('fs', 'tp')
- gate_sampler: bfloat16 [8, 4096, 4096], P('tp', None, 'fs')
- up_sampler: bfloat16 [8, 4096, 4096], P('tp', None, 'fs')
- down_sampler: bfloat16 [8, 4096, 4096], P('tp', None, 'fs')
Inputs may be any that keep to these rules, and one draw needn't show every extreme that they name: `routes`: the 2 experts of a token differ. Within the tokens of one index of fs (aligned blocks of 40 rows) no expert is named by more than 30 tokens.
All inputs are finite; a program needn't handle non-finite values.
Results may differ from a plain program's by a relative error of at most 0.01.
Values may be sent and summed in bfloat16 or wider, within the bound.
A program may use at most 128 MiB of HBM per device.

v0:
```python
import jax
import jax.numpy as jnp
from jax import lax
from jax.sharding import PartitionSpec as P

CAP = 30


def in_one_piece(arrays, axis, split_dim, concat_dim, along):
    both = jnp.concatenate(arrays, axis=along)
    out, at, gathered = (
        lax.all_to_all(both, axis, split_axis=split_dim, concat_axis=concat_dim, tiled=True),
        0,
        [],
    )
    for a in arrays:
        gathered.append(lax.slice_in_dim(out, at, at + a.shape[along], axis=along))
        at += a.shape[along]
    return tuple(gathered)


def joined_along(parts, dim):
    shape = list(parts.shape[1:])
    shape[dim] *= parts.shape[0]
    return jnp.moveaxis(parts, 0, dim).reshape(shape)


def from_everyone(shard, axis):
    copies = jnp.broadcast_to(shard, (lax.axis_size(axis), *shard.shape))
    return lax.all_to_all(copies, axis, split_axis=0, concat_axis=0, tiled=True)


def gathered_copies(shard, axis, dim):
    return joined_along(from_everyone(shard, axis), dim)


def arrange(matrix, spread):
    experts, width, columns = matrix.shape
    block = columns // spread
    split = matrix.reshape(experts, width, spread, block)
    return jnp.transpose(split, (0, 2, 1, 3)).reshape(experts * spread, width, block)


def outgoing_rows(placing, row_data, experts, spread):
    packed = jnp.einsum(
        "rec,rd->ecd", placing.astype(jnp.bfloat16), row_data, preferred_element_type=jnp.float32
    ).astype(jnp.bfloat16)
    copies = jnp.broadcast_to(packed[:, None], (experts, spread) + packed.shape[1:])
    return copies.reshape((experts * spread,) + packed.shape[1:])


def per_device(tokens, routes, route_logits, norm_gain, gate_weight, up_weight, down_weight):
    experts = gate_weight.shape[0]
    fs_count = lax.axis_size("fs")
    spread = fs_count // experts
    gain_cols = norm_gain[None, :, None]
    gate_pieces = arrange((gate_weight * gain_cols).astype(jnp.bfloat16), spread)
    up_pieces = arrange((up_weight * gain_cols).astype(jnp.bfloat16), spread)
    down_pieces = arrange(down_weight.astype(jnp.bfloat16), spread)
    gate_local, up_local, down_local = in_one_piece(
        (gate_pieces, up_pieces, down_pieces), "fs", 0, 1, 2
    )
    gate_matrix = gate_local[0]
    up_matrix = up_local[0]
    down_matrix = down_local[0]
    tok_float = tokens.astype(jnp.float32)
    normed = (
        tok_float * lax.rsqrt(jnp.mean(tok_float * tok_float, axis=1, keepdims=True) + 1e-05)
    ).astype(jnp.bfloat16)
    shares = jax.nn.sigmoid(route_logits - route_logits[:, ::-1])
    expert_ids = lax.broadcasted_iota(jnp.int32, (1, 1, experts), 2)
    picks = (routes[:, :, None] == expert_ids).astype(jnp.int32)
    member = jnp.sum(picks, axis=1)
    position = jnp.cumsum(member, axis=0) - member
    slot_ids = lax.broadcasted_iota(jnp.int32, (1, 1, CAP), 2)
    placing = ((position[:, :, None] == slot_ids) & (member[:, :, None] > 0)).astype(jnp.float32)
    weights = jnp.sum(picks.astype(jnp.float32) * shares[:, :, None], axis=1)
    combine = jnp.transpose(placing * weights[:, :, None], (1, 2, 0))
    cols_out = gate_matrix.shape[1]
    part_width = normed.shape[1] // lax.axis_size("tp")
    own_cols = lax.dynamic_slice_in_dim(normed, lax.axis_index("tp") * part_width, part_width, 1)
    sending = outgoing_rows(placing, own_cols, experts, spread)
    arrived = lax.all_to_all(sending, "fs", split_axis=0, concat_axis=0, tiled=True)
    segment = lax.all_gather(arrived, "tp", axis=2, tiled=True)
    flat_rows = segment.reshape(-1, segment.shape[2])
    gate_act = jnp.dot(flat_rows, gate_matrix, preferred_element_type=jnp.float32)
    up_act = jnp.dot(flat_rows, up_matrix, preferred_element_type=jnp.float32)
    hidden = (
        (jax.nn.silu(gate_act) * up_act)
        .astype(jnp.bfloat16)
        .reshape(arrived.shape[0], arrived.shape[1], cols_out)
    )
    slot_rows = hidden.reshape(-1, cols_out)
    down_group = lax.all_to_all(down_matrix, "tp", split_axis=0, concat_axis=1, tiled=True)
    summed = lax.dot_general(
        down_group,
        gathered_copies(slot_rows, "tp", 1),
        (((1,), (1,)), ((), ())),
        preferred_element_type=jnp.float32,
    )
    back = lax.all_to_all(
        summed.reshape(summed.shape[0], fs_count, CAP).astype(jnp.bfloat16),
        "fs",
        split_axis=1,
        concat_axis=1,
        tiled=True,
    ).astype(jnp.float32)
    per_expert = jnp.sum(back.reshape(back.shape[0], experts, spread, CAP), axis=2)
    mixed = jnp.einsum("dec,ecr->rd", per_expert, combine, precision=lax.Precision.HIGHEST).astype(
        jnp.bfloat16
    )
    return (mixed, gate_local, up_local, down_local)


def solution(mesh):
    in_specs = (
        P("fs", None),
        P("fs", None),
        P("fs", None),
        P("fs"),
        P(None, "fs", "tp"),
        P(None, "fs", "tp"),
        P(None, "fs", "tp"),
    )
    out_specs = (P("fs", "tp"), P("tp", None, "fs"), P("tp", None, "fs"), P("tp", None, "fs"))
    return jax.shard_map(
        per_device, mesh=mesh, in_specs=in_specs, out_specs=out_specs, check_vma=False
    )
```

profile of v0, /device:TPU:1, one launch (start us, length us, event | category | flops | bytes accessed | tf_op | source)
XLA Modules:
  0.0 236.4 jit_solution(16118787608043097368)
XLA Ops:
  7.2 0.0 copy-start.3
  7.2 0.0 all-gather.2.cloned.1.call-start
  7.2 0.8 convert_reduce_fusion.1
  8.1 0.1 copy.47
  8.2 1.1 multiply_reduce_fusion
  9.3 1.0 convert_element_type.47
  10.3 0.1 reduce_window_sum.11
  10.4 0.1 copy.54
  10.5 0.2 convolution_convert_fusion
  10.7 0.1 broadcast_in_dim.4
  10.9 38.0 %all_to_all.46 = bf16[32,30,512]{2,1,0:T(8,128)(2,1)} all-to-all(bf16[32,30,512]{2,1,0:T(8,128)(2,1)S(1)} %bitcast.62), channel_id=1, replica_groups=mesh['fs'=32,'tp'=8] {'fs'}, dimensions={0} | all-to-all | bytes 1966080 | tf_op jit(solution)/shard_map/all_to_all | solution.py:83
  48.8 0.0 all-gather.2.cloned.1.call-update
  48.8 0.0 copy-done.3
  48.9 0.2 convert_element_type.44
  49.0 0.0 copy-start.1
  49.0 0.0 copy-start.2
  49.0 0.0 copy-start.8
  49.0 0.3 copy.63
  49.3 0.1 bitcast_bitcast_fusion
  49.4 0.2 copy.52
  49.6 1.0 copy-done.1
  50.6 0.6 copy-done.2
  51.2 0.0 copy-done.8
  51.2 0.7 multiply_convert_fusion.1
  51.9 0.3 copy.61
  52.2 0.1 bitcast_bitcast_fusion.2
  52.3 0.2 copy.50
  52.5 0.3 copy.62
  52.8 0.1 bitcast_bitcast_fusion.1
  52.9 0.2 copy.51
  53.1 0.5 pad_maximum_fusion
  53.6 76.5 %all_to_all.47 = bf16[32,128,384]{2,1,0:T(8,128)(2,1)S(1)} all-to-all(bf16[32,128,384]{2,1,0:T(8,128)(2,1)S(1)} %pad_maximum_fusion), channel_id=1, replica_groups=mesh['fs'=32,'tp'=8] {'fs'}, dimensions={0} | all-to-all | bytes 6291456 | tf_op jit(solution)/shard_map/all_to_all | solution.py:12
  130.1 1.9 fusion.28
  132.0 0.0 copy-start.4
  132.0 8.1 %all-to-all-start.1 = ((bf16[8,512,128]{2,1,0:T(8,128)(2,1)}), bf16[8,512,128]{2,1,0:T(8,128)(2,1)S(1)}, u32[]{:S(2)}, u32[]{:S(2)}) async-start(bf16[8,512,128]{2,1,0:T(8,128)(2,1)} %bitcast.10), calls=%async_computation.1 | async-start | bytes 2097152 | tf_op jit(solution)/shard_map/all_to_all | solution.py:94
  140.1 0.0 all-gather.2.cloned.1.call-done
  140.1 9.5 %reshape.82 = bf16[960,4096]{1,0:T(8,128)(2,1)} reshape(bf16[32,30,4096]{2,1,0:T(8,128)(2,1)} %all-gather.2.cloned.1.call-done) | data formatting | bytes 15728640 | tf_op jit(solution)/shard_map/reshape | solution.py:85
  149.6 0.0 copy-done.4
  149.6 0.0 copy-start
  149.6 0.0 copy-start.5
  149.6 5.6 %fusion.8 = f32[960,128]{1,0:T(8,128)S(1)} fusion(bf16[960,4096]{1,0:T(8,128)(2,1)} %reshape.82, bf16[1,4096,128]{2,1,0:T(8,128)(2,1)S(1)} %get-tuple-element.4), kind=kOutput, calls=%fused_computation.16 | convolution fusion | flops 1006632960 | bytes 9404416 | tf_op jit(solution)/shard_map/dot_general | solution.py:86
  155.2 0.0 copy-done
  155.2 0.1 copy-done.5
  155.3 2.2 fusion.5
  157.5 0.0 all-to-all-done.1
  157.5 1.6 broadcast_in_dim.5
  159.0 4.8 %all-to-all-start.3 = ((bf16[8,960,128]{2,1,0:T(8,128)(2,1)}), bf16[8,960,128]{2,1,0:T(8,128)(2,1)S(1)}, u32[]{:S(2)}, u32[]{:S(2)}) async-start(bf16[8,960,128]{2,1,0:T(8,128)(2,1)} %broadcast_in_dim.5), calls=%async_computation.3 | async-start | bytes 3932160 | tf_op jit(solution)/shard_map/all_to_all | solution.py:30
  163.8 1.7 copy.53
  165.5 1.5 reshape.88
  167.0 21.6 %all-to-all-done.3 = bf16[8,960,128]{2,1,0:T(8,128)(2,1)S(1)} async-done(((bf16[8,960,128]{2,1,0:T(8,128)(2,1)}), bf16[8,960,128]{2,1,0:T(8,128)(2,1)S(1)}, u32[]{:S(2)}, u32[]{:S(2)}) %all-to-all-start.3) | async-done | bytes 1966112 | tf_op jit(solution)/shard_map/all_to_all | solution.py:30
  188.6 2.6 %copy.55 = bf16[960,8,128]{2,1,0:T(8,128)(2,1)} copy(bf16[960,8,128]{2,0,1:T(8,128)(2,1)S(1)} %bitcast.57) | data formatting | bytes 3932160 | tf_op jit(solution)/shard_map/transpose | solution.py:25
  191.2 3.0 %dot_general.20 = bf16[32,30,1024]{2,1,0:T(8,128)(2,1)S(1)} reshape(bf16[960,8,128]{2,1,0:T(8,128)(2,1)} %copy.55) | data formatting | bytes 3932160 | tf_op jit(solution)/shard_map/dot_general | solution.py:95
  194.2 1.4 fusion.2
  195.6 0.0 copy-start.6
  195.6 0.0 copy-start.7
  195.6 1.5 copy.57
  197.1 5.3 %all-to-all-start.4 = ((bf16[512,32,30]{0,2,1:T(8,128)(2,1)}), bf16[512,32,30]{0,2,1:T(8,128)(2,1)S(1)}, u32[]{:S(2)}, u32[]{:S(2)}) async-start(bf16[512,32,30]{0,2,1:T(8,128)(2,1)} %copy.57), calls=%async_computation.4 | async-start | bytes 2097152 | tf_op jit(solution)/shard_map/all_to_all | solution.py:101
  202.5 0.0 copy-done.6
  202.5 0.1 copy.49
  202.6 0.0 copy-done.7
  202.6 25.9 %all-to-all-done.4 = bf16[512,32,30]{0,2,1:T(8,128)(2,1)S(1)} async-done(((bf16[512,32,30]{0,2,1:T(8,128)(2,1)}), bf16[512,32,30]{0,2,1:T(8,128)(2,1)S(1)}, u32[]{:S(2)}, u32[]{:S(2)}) %all-to-all-start.4) | async-done | bytes 983072 | tf_op jit(solution)/shard_map/all_to_all | solution.py:101
  228.5 0.2 convert_reduce_fusion
  228.7 0.9 fusion.6
  (7 shorter events, 0.1 us)
Async XLA Ops:
  7.2 41.7 %copy-start.3 = (f32[4,128,1024]{2,1,0:T(8,128)S(1)}, f32[4,128,1024]{2,1,0:T(8,128)}, u32[]{:S(2)}) copy-start(f32[4,128,1024]{2,1,0:T(8,128)} %param.13) | copy-start | bytes 6291460
  7.2 132.9 %all-gather.2.cloned.1.call-start = ((), (), s32[]{:S(2)}) async-start(), calls=%async_computation.5 | async-start | bytes 9437184 | tf_op jit(solution)/shard_map/all_gather | solution.py:84
  49.0 1.6 copy-start.1
  49.0 2.2 copy-start.2
  49.0 2.2 copy-start.8
  132.0 17.6 %copy-start.4 = (bf16[1,4096,128]{2,1,0:T(8,128)(2,1)}, bf16[1,4096,128]{2,1,0:T(8,128)(2,1)S(1)}, u32[]{:S(2)}) copy-start(bf16[1,4096,128]{2,1,0:T(8,128)(2,1)S(1)} %get-tuple-element.4) | copy-start | bytes 3145732
  132.0 25.5 %all-to-all-start.1 = ((bf16[8,512,128]{2,1,0:T(8,128)(2,1)}), bf16[8,512,128]{2,1,0:T(8,128)(2,1)S(1)}, u32[]{:S(2)}, u32[]{:S(2)}) async-start(bf16[8,512,128]{2,1,0:T(8,128)(2,1)} %bitcast.10), calls=%async_computation.1 | async-start | bytes 2097152 | tf_op jit(solution)/shard_map/all_to_all | solution.py:94
  149.6 5.6 %copy-start = (bf16[960,4096]{1,0:T(8,128)(2,1)S(1)}, bf16[960,4096]{1,0:T(8,128)(2,1)}, u32[]{:S(2)}) copy-start(bf16[960,4096]{1,0:T(8,128)(2,1)} %reshape.82) | copy-start | bytes 23592964
  149.6 5.7 %copy-start.5 = (bf16[1,4096,128]{2,1,0:T(8,128)(2,1)S(1)}, bf16[1,4096,128]{2,1,0:T(8,128)(2,1)}, u32[]{:S(2)}) copy-start(bf16[1,4096,128]{2,1,0:T(8,128)(2,1)} %get-tuple-element.5) | copy-start | bytes 3145732
  159.0 29.6 %all-to-all-start.3 = ((bf16[8,960,128]{2,1,0:T(8,128)(2,1)}), bf16[8,960,128]{2,1,0:T(8,128)(2,1)S(1)}, u32[]{:S(2)}, u32[]{:S(2)}) async-start(bf16[8,960,128]{2,1,0:T(8,128)(2,1)} %broadcast_in_dim.5), calls=%async_computation.3 | async-start | bytes 3932160 | tf_op jit(solution)/shard_map/all_to_all | solution.py:30
  195.6 6.9 %copy-start.6 = (f32[40,2]{0,1:T(2,128)S(1)}, f32[40,2]{0,1:T(2,128)}, u32[]{:S(2)}) copy-start(f32[40,2]{0,1:T(2,128)} %param.9) | copy-start | bytes 964
  195.6 7.0 %copy-start.7 = (s32[40,2]{0,1:T(2,128)S(1)}, s32[40,2]{0,1:T(2,128)}, u32[]{:S(2)}) copy-start(s32[40,2]{0,1:T(2,128)} %param.8) | copy-start | bytes 964
  197.1 31.3 %all-to-all-start.4 = ((bf16[512,32,30]{0,2,1:T(8,128)(2,1)}), bf16[512,32,30]{0,2,1:T(8,128)(2,1)S(1)}, u32[]{:S(2)}, u32[]{:S(2)}) async-start(bf16[512,32,30]{0,2,1:T(8,128)(2,1)} %copy.57), calls=%async_computation.4 | async-start | bytes 2097152 | tf_op jit(solution)/shard_map/all_to_all | solution.py:101
Sparse Core Ops, SparseCore 0:
  49.0 51.9 all-gather.1
where the time goes:
time: 239 us; the launch traced here: 236 us
  blocking collectives  114 us (48%)
  waiting for transfers between devices  47.5 us (20%)
  local copies, waits for them, and re-layouts  27.1 us (11%)
  starting transfers between devices  18.2 us (8%)
  between operations  14.3 us (6%)
  matrix products  10.3 us (4%)
  other arithmetic  4.59 us (2%)
    all_to_all x1, blocking collectives, in_one_piece(): lax.all_to_all(both, axis, split_axis=split_dim, concat_axis=concat_dim,...  76.5 us
    all_to_all x1, blocking collectives, per_device(): lax.all_to_all(sending, 'fs', split_axis=0, concat_axis=0, tiled=True)  38 us
    all_to_all x1, waiting for transfers between devices, per_device(): lax.all_to_all(summed.reshape(summed.shape[0], fs_count, CAP).astype(jnp....  25.9 us
    all_to_all x1, waiting for transfers between devices, from_everyone(): return lax.all_to_all(copies, axis, split_axis=0, concat_axis=0, tiled=True)  21.6 us
    reshape x1, local copies, waits for them, and re-layouts, per_device(): flat_rows = segment.reshape(-1, segment.shape[2])  9.51 us
    all_to_all x1, starting transfers between devices, per_device(): lax.all_to_all(down_matrix, 'tp', split_axis=0, concat_axis=1, tiled=True)  8.06 us
    dot_general x1, matrix products, per_device(): jnp.dot(flat_rows, gate_matrix, preferred_element_type=jnp.float32)  5.57 us
    all_to_all x1, starting transfers between devices, per_device(): lax.all_to_all(summed.reshape(summed.shape[0], fs_count, CAP).astype(jnp....  5.31 us
  transfers between devices with their start and end apart: 4, of which 2 were waited for; matrix products, arithmetic and copies ran while one was open for 11% of the time, Pallas kernels for 0%

commit v1 on v0

v1 whole, which is shorter than its diff:
```python
import functools

import jax
import jax.numpy as jnp
from jax import lax
from jax.experimental import pallas as pl
from jax.experimental.pallas import tpu as pltpu
from jax.sharding import PartitionSpec as P

MESH = pl.DeviceIdType.MESH
NZ, NX, NY = 8, 4, 4
NFS, NTP = 32, 8
EXPERTS = 4
D = 4096
KB = D // NTP
TOK = 40
SLOT = 32
ROWS = NFS * SLOT
XROWS = NZ * SLOT
NC = 4
DR = 128 // NC
CW = NX * DR
F32, BF16 = jnp.float32, jnp.bfloat16


def rem(a, n):
    return lax.rem(a, jnp.int32(n))


def div(a, n):
    return lax.div(a, jnp.int32(n))


def kernel(
    tok_hbm, routes_ref, logits_ref, gain_ref, gate_hbm, up_hbm, down_hbm,
    mixed_ref, gate_out, up_out, down_out,
    tok, stage, wmix, p_send, sg, sd, wgu, wd, xg, hid, dn, ro, r1, r2, rr,
    tok_sem, load_sem,
    t1_s, t1_r, t2_s, t2_r, t3_s, t3_r, t3f_s, cc_s, cc_r,
    gu_s, gu_r, wd_s, wd_r, h_s, h_r, hc_s, hc_r, dn_s, dn_r, r1_s, r1_r, r2_s, r2_r,
    out_sem, outd_sem,
):
    fs, tp = lax.axis_index("fs"), lax.axis_index("tp")
    z, x = div(fs, NX), rem(fs, NX)
    y, core = div(tp, 2), rem(tp, 2)

    def rcopy(src, dst, ssem, rsem, fs2, tp2):
        return pltpu.make_async_remote_copy(
            src_ref=src, dst_ref=dst, send_sem=ssem, recv_sem=rsem,
            device_id=(fs2, tp2), device_id_type=MESH,
        )

    def wait_for(sem, ref):
        pltpu.make_async_copy(ref, ref, sem).wait()

    def tp_of(dy):
        return rem(y + dy, NY) * 2 + core

    other = y * 2 + (1 - core)

    bar = pltpu.get_barrier_semaphore()

    @pl.loop(1, NFS)
    def _(i):
        pl.semaphore_signal(bar, inc=1, device_id=(rem(fs + i, NFS), tp), device_id_type=MESH)

    @pl.loop(1, NTP)
    def _(i):
        pl.semaphore_signal(bar, inc=1, device_id=(fs, rem(tp + i, NTP)), device_id_type=MESH)

    tok_copy = pltpu.make_async_copy(tok_hbm, tok, tok_sem)
    tok_copy.start()
    loads = []
    for m, hbm in enumerate((gate_hbm, up_hbm, down_hbm)):
        cp = pltpu.make_async_copy(hbm, stage.at[m], load_sem.at[m])
        cp.start()
        loads.append(cp)

    lane = lax.broadcasted_iota(jnp.int32, (TOK, EXPERTS * SLOT), 1)
    lane_e = div(lane, SLOT)
    lane_s = rem(lane, SLOT).astype(F32)
    pick0 = jnp.where(routes_ref[:, 0:1] == lane_e, 1.0, 0.0).astype(F32)
    pick1 = jnp.where(routes_ref[:, 1:2] == lane_e, 1.0, 0.0).astype(F32)
    member = pick0 + pick1
    row_i = lax.broadcasted_iota(jnp.int32, (TOK, TOK), 0)
    col_i = lax.broadcasted_iota(jnp.int32, (TOK, TOK), 1)
    before = jnp.where(col_i < row_i, 1.0, 0.0).astype(BF16)
    position = jnp.dot(before, member.astype(BF16), preferred_element_type=F32)
    placing = jnp.where((position == lane_s) & (member > 0.0), 1.0, 0.0).astype(F32)
    diff = logits_ref[:, 0:1] - logits_ref[:, 1:2]
    share0 = 1.0 / (1.0 + jnp.exp(-diff))
    share1 = 1.0 / (1.0 + jnp.exp(diff))
    wmix[...] = placing * (pick0 * share0 + pick1 * share1)

    tok_copy.wait()
    tf = tok[...].astype(F32)
    inv = lax.rsqrt(jnp.mean(tf * tf, axis=1, keepdims=True) + 1e-05)
    block = tok[:, pl.ds(pl.multiple_of(tp * KB, KB), KB)].astype(F32)
    normed = (block * inv).astype(BF16)
    packed = lax.dot_general(
        placing.astype(BF16), normed, (((0,), (0,)), ((), ())), preferred_element_type=F32
    )
    p_send[...] = packed.astype(BF16).reshape(EXPERTS, SLOT, KB)
    own_x = pl.multiple_of(x * XROWS, XROWS)
    own_row = pl.multiple_of(x * XROWS + z * SLOT, SLOT)
    xg[tp, pl.ds(own_row, SLOT), :] = p_send[div(z, 2)]

    gain = jnp.transpose(jnp.broadcast_to(gain_ref[...], (128, 128)))
    for m in range(2):
        loads[m].wait()

        @pl.loop(0, EXPERTS)
        def _(e):
            for s in range(8):
                sg[e * 8 + s, :, m * 128 : (m + 1) * 128] = (
                    stage[m, e, :, s * 128 : (s + 1) * 128] * gain
                ).astype(BF16)

    wgu[pl.ds(pl.multiple_of(fs * 128, 128), 128), :] = sg[fs]

    pl.semaphore_wait(bar, NFS - 1 + NTP - 1)

    @pl.loop(1, NZ)
    def _(dz):
        z2 = rem(z + dz, NZ)
        rcopy(
            p_send.at[div(z2, 2)], xg.at[tp, pl.ds(own_row, SLOT), :], t1_s, t1_r, z2 * NX + x, tp
        ).start()

    my_rows = pl.ds(pl.multiple_of(fs * 128, 128), 128)

    def send_gu(dz, dx):
        f2 = rem(z + dz, NZ) * NX + rem(x + dx, NX)
        rcopy(sg.at[f2], wgu.at[my_rows, :], gu_s, gu_r, f2, tp).start()

    def send_down(k, i):
        dx, dz = div(i, NZ), rem(i, NZ)
        f2 = rem(z + dz, NZ) * NX + rem(x + dx, NX)
        part = pl.ds(k * DR, DR)
        rcopy(
            sd.at[f2, part, :], wd.at[z, x, part, :], wd_s.at[k], wd_r.at[k], f2, tp
        ).start()

    @pl.loop(1, NZ)
    def _(dz):
        send_gu(dz, 0)

    loads[2].wait()

    @pl.loop(0, EXPERTS)
    def _(e):
        for s in range(8):
            sd[e * 8 + s] = stage[2, e, :, s * 128 : (s + 1) * 128].astype(BF16)

    wd[z, x] = sd[fs]

    wait_for(t1_r, xg.at[0, 0 : (NZ - 1) * SLOT, :])
    mine = xg.at[tp, pl.ds(own_x, XROWS), :]
    t2 = []
    for dx in range(1, NX):
        cp = rcopy(mine, mine, t2_s.at[dx - 1], t2_r.at[dx - 1], z * NX + rem(x + dx, NX), tp)
        cp.start()
        t2.append(cp)

    def part_of(t, p, half=None):
        base = rem(x + NX - p, NX) * XROWS
        if half is None:
            return xg.at[t, pl.ds(pl.multiple_of(base, XROWS), XROWS), :]
        h = XROWS // 2
        return xg.at[t, pl.ds(pl.multiple_of(base + half * h, h), h), :]

    def to_core(t, p):
        ref = part_of(t, p)
        rcopy(ref, ref, cc_s, cc_r, fs, other).start()

    def own_part(p):
        ref = part_of(tp, p)
        rcopy(ref, ref, t3_s, t3_r.at[0, p], fs, tp_of(1)).start()
        rcopy(ref, ref, t3_s, t3_r.at[1, p], fs, tp_of(3)).start()
        to_core(tp, p)

    own_part(0)

    @pl.loop(0, 3 * NZ)
    def _(i):
        send_gu(rem(i, NZ), 1 + div(i, NZ))

    for k in range(min(2, NC)):

        @pl.loop(1, NFS)
        def _(i):
            send_down(k, i)

    for p in range(1, NX):
        t2[p - 1].wait_recv()
        own_part(p)

    for p in range(NX):
        below, above = tp_of(3), tp_of(1)
        ref = part_of(below, p)
        wait_for(t3_r.at[0, p], ref)
        half = part_of(below, p, 0)
        rcopy(half, half, t3f_s, t3_r.at[2, p], fs, above).start()
        to_core(below, p)
        ref = part_of(above, p)
        wait_for(t3_r.at[1, p], ref)
        half = part_of(above, p, 1)
        rcopy(half, half, t3f_s, t3_r.at[2, p], fs, below).start()
        to_core(above, p)
    for p in range(NX):
        wait_for(t3_r.at[2, p], part_of(tp_of(2), p))
        to_core(tp_of(2), p)
    wait_for(cc_r, xg.at[0:NY])
    wait_for(gu_r, wgu.at[0 : (NFS - 1) * 128, :])

    outs = [
        pltpu.make_async_copy(wgu.at[:, 0:128], gate_out, out_sem.at[0]),
        pltpu.make_async_copy(wgu.at[:, 128:256], up_out, out_sem.at[1]),
    ]
    for cp in outs:
        cp.start()

    my_lanes = pl.ds(pl.multiple_of(tp * 128, 128), 128)

    @pl.loop(0, NX)
    def _(r):
        rows = pl.ds(pl.multiple_of(r * XROWS, XROWS), XROWS)
        acc = jnp.zeros((XROWS, 256), F32)
        for t in range(NTP):
            acc += jnp.dot(
                xg[t, rows, :], wgu[t * KB : (t + 1) * KB, :], preferred_element_type=F32
            )
        g, u = acc[:, 0:128], acc[:, 128:256]
        hid[rows, my_lanes] = (g / (1.0 + jnp.exp(-g)) * u).astype(BF16)

    def lanes_of(t):
        return hid.at[:, pl.ds(pl.multiple_of(t * 128, 128), 128)]

    own_h = lanes_of(tp)
    for dy in (1, 3, 2):
        rcopy(own_h, own_h, h_s, h_r.at[dy - 1], fs, tp_of(dy)).start()
    rcopy(own_h, own_h, hc_s, hc_r, fs, other).start()
    for dy in (1, 3, 2):
        ref = lanes_of(tp_of(NY - dy))
        wait_for(h_r.at[dy - 1], ref)
        rcopy(ref, ref, hc_s, hc_r, fs, other).start()
    wait_for(hc_r, hid.at[:, 0 : NY * 128])

    def summed(k):
        wait_for(r1_r.at[k], r1.at[k])
        total = ro[k, x].astype(F32)
        for i in range(NX - 1):
            total += r1[k, i].astype(F32)
        r2[k] = total.astype(BF16).reshape(NZ, SLOT, CW)
        cols = slice(k * CW, (k + 1) * CW)
        rr[z, :, cols] = r2[k, z]

        @pl.loop(1, NZ)
        def _(dz):
            z2 = rem(z + dz, NZ)
            rcopy(
                r2.at[k, z2], rr.at[z, :, cols], r2_s.at[k], r2_r.at[k], z2 * NX + x, tp
            ).start()

    out_down = []
    for k in range(NC):
        part = slice(k * DR, (k + 1) * DR)
        wait_for(wd_r.at[k], sd.at[0 : NFS - 1, 0:DR, :])
        if k + 2 < NC:

            @pl.loop(1, NFS)
            def _(i):
                send_down(k + 2, i)

        @pl.loop(1, NTP)
        def _(i):
            t2_ = rem(tp + i, NTP)
            rcopy(
                wd.at[t2_, :, part, :], dn.at[k, :, :, my_lanes], dn_s.at[k], dn_r.at[k], fs, t2_
            ).start()

        dn[k, :, :, my_lanes] = wd[tp, :, part, :]
        cp = pltpu.make_async_copy(wd.at[:, :, part, :], down_out.at[:, :, part, :], outd_sem.at[k])
        cp.start()
        out_down.append(cp)
        wait_for(dn_r.at[k], sd.at[0 : 4 * (NTP - 1), 0:DR, :])
        dnk = dn[k].reshape(CW, NTP * 128)
        for j in (1, 2, 3, 0):
            x2 = rem(x + j, NX)
            rows = pl.ds(pl.multiple_of(x2 * XROWS, XROWS), XROWS)
            ro[k, x2] = lax.dot_general(
                hid[rows, :], dnk, (((1,), (1,)), ((), ())), preferred_element_type=F32
            ).astype(BF16)
        for j in (1, 2, 3):
            x2 = rem(x + j, NX)
            rcopy(
                ro.at[k, x2], r1.at[k, j - 1], r1_s.at[k], r1_r.at[k], z * NX + x2, tp
            ).start()
        if k >= 1:
            summed(k - 1)
    summed(NC - 1)

    for k in range(NC):
        wait_for(r2_r.at[k], r2.at[k, 0 : NZ - 1])
    got = rr[...].astype(F32)
    per_expert = jnp.concatenate([got[2 * e] + got[2 * e + 1] for e in range(EXPERTS)], axis=0)
    mixed_ref[...] = jnp.dot(
        wmix[...], per_expert, precision=lax.Precision.HIGHEST, preferred_element_type=F32
    ).astype(BF16)

    wait_for(t1_s, xg.at[0, 0 : (NZ - 1) * SLOT, :])
    for cp in t2:
        cp.wait_send()
    wait_for(t3_s, xg.at[0:2])
    wait_for(t3f_s, xg.at[0])
    wait_for(cc_s, xg.at[0:NY])
    wait_for(gu_s, wgu.at[0 : (NFS - 1) * 128, :])
    wait_for(h_s, hid.at[:, 0 : (NY - 1) * 128])
    wait_for(hc_s, hid.at[:, 0 : NY * 128])
    for k in range(NC):
        wait_for(wd_s.at[k], sd.at[0 : NFS - 1, 0:DR, :])
        wait_for(dn_s.at[k], sd.at[0 : 4 * (NTP - 1), 0:DR, :])
        wait_for(r1_s.at[k], r1.at[k])
        wait_for(r2_s.at[k], r2.at[k, 0 : NZ - 1])
    for cp in outs + out_down:
        cp.wait()


def per_device(tokens, routes, route_logits, norm_gain, gate_weight, up_weight, down_weight):
    dma = pltpu.SemaphoreType.DMA
    hbm = pl.BlockSpec(memory_space=pl.ANY)
    vmem = pl.BlockSpec(memory_space=pltpu.VMEM)
    mixed, gate, up, down = pl.pallas_call(
        kernel,
        out_shape=(
            jax.ShapeDtypeStruct((TOK, KB), BF16),
            jax.ShapeDtypeStruct((D, 128), BF16),
            jax.ShapeDtypeStruct((D, 128), BF16),
            jax.ShapeDtypeStruct((NZ, NX, 128, 128), BF16),
        ),
        in_specs=[hbm, vmem, vmem, vmem, hbm, hbm, hbm],
        out_specs=(vmem, hbm, hbm, hbm),
        scratch_shapes=[
            pltpu.VMEM((TOK, D), BF16),
            pltpu.VMEM((3, EXPERTS, 128, 1024), F32),
            pltpu.VMEM((TOK, EXPERTS * SLOT), F32),
            pltpu.VMEM((EXPERTS, SLOT, KB), BF16),
            pltpu.VMEM((NFS, 128, 256), BF16),
            pltpu.VMEM((NFS, 128, 128), BF16),
            pltpu.VMEM((D, 256), BF16),
            pltpu.VMEM((NZ, NX, 128, 128), BF16),
            pltpu.VMEM((NTP, ROWS, KB), BF16),
            pltpu.VMEM((ROWS, NTP * 128), BF16),
            pltpu.VMEM((NC, NX, DR, NTP * 128), BF16),
            pltpu.VMEM((NC, NX, XROWS, CW), BF16),
            pltpu.VMEM((NC, NX - 1, XROWS, CW), BF16),
            pltpu.VMEM((NC, NZ, SLOT, CW), BF16),
            pltpu.VMEM((NZ, SLOT, KB), BF16),
            dma, dma((3,)),
            dma, dma, dma((NX - 1,)), dma((NX - 1,)), dma, dma((3, NX)), dma, dma, dma,
            dma, dma, dma((NC,)), dma((NC,)), dma, dma((NY - 1,)), dma, dma,
            dma((NC,)), dma((NC,)), dma((NC,)), dma((NC,)), dma((NC,)), dma((NC,)),
            dma((2,)), dma((NC,)),
        ],
        compiler_params=pltpu.CompilerParams(
            collective_id=0, has_side_effects=True, vmem_limit_bytes=56 * 2**20
        ),
        name="expert_handover",
    )(tokens, routes, route_logits, norm_gain[None, :], gate_weight, up_weight, down_weight)
    mixed = mixed.reshape(TOK, NC, NX, DR).transpose(0, 2, 1, 3).reshape(TOK, KB)
    return (mixed, gate[None], up[None], down.reshape(1, D, 128))


def solution(mesh):
    in_specs = (
        P("fs", None),
        P("fs", None),
        P("fs", None),
        P("fs"),
        P(None, "fs", "tp"),
        P(None, "fs", "tp"),
        P(None, "fs", "tp"),
    )
    out_specs = (P("fs", "tp"), P("tp", None, "fs"), P("tp", None, "fs"), P("tp", None, "fs"))
    return jax.shard_map(
        per_device, mesh=mesh, in_specs=in_specs, out_specs=out_specs, check_vma=False
    )
```

time: 239 us -> 133 us (0.56)
  Pallas kernels: 0 us -> 123 us
  blocking collectives: 114 us -> 0 us
  waiting for transfers between devices: 47.5 us -> 0 us
  starting transfers between devices: 18.2 us -> 0 us
  local copies, waits for them, and re-layouts: 27.1 us -> 8.92 us
  between operations: 14.3 us -> 0.67 us
  matrix products: 10.3 us -> 0 us
  other arithmetic: 4.59 us -> 0 us
    pallas_call x0 -> x1, Pallas kernels: none -> 123 us  [per_device(): pl.pallas_call(kernel, out_shape=(jax.ShapeDtypeStruct((TOK, KB), BF16),...]
    all_to_all x2 -> x0, blocking collectives: 114 us -> none  [the longest x1 76.5 us: in_one_piece(): lax.all_to_all(both, axis, split_axis=split_dim, concat_axis=concat_dim,...]
    all_to_all x3 -> x0, waiting for transfers between devices: 47.5 us -> none  [the longest x1 25.9 us: per_device(): lax.all_to_all(summed.reshape(summed.shape[0], fs_count, CAP).astype(jnp....]
    all_to_all x3 -> x0, starting transfers between devices: 18.2 us -> none  [the longest x1 8.06 us: per_device(): lax.all_to_all(down_matrix, 'tp', split_axis=0, concat_axis=1, tiled=True)]
    dot_general x5 -> x0, matrix products: 10.3 us -> none  [the longest x1 5.57 us: per_device(): jnp.dot(flat_rows, gate_matrix, preferred_element_type=jnp.float32)]
    reshape x1 -> x2, local copies, waits for them, and re-layouts: 9.51 us -> 1.82 us  [per_device(): mixed.reshape(TOK, NC, NX, DR).transpose(0, 2, 1, 3).reshape(TOK, KB)]
    unnamed x21 -> x9, local copies, waits for them, and re-layouts: 2.54 us -> 7.03 us
    transpose x7 -> x1, local copies, waits for them, and re-layouts: 3.5 us -> 0.06 us  [per_device(): mixed.reshape(TOK, NC, NX, DR).transpose(0, 2, 1, 3).reshape(TOK, KB)]
  transfers between devices with their start and end apart: 4 -> 0, of which waited for: 2 -> 0; matrix products, arithmetic and copies ran while one was open for 11% -> 0% of each run, Pallas kernels for 0% -> 0%
where the time goes in v1:
time: 133 us; the launch traced here: 132 us
  Pallas kernels  123 us (92%)
  local copies, waits for them, and re-layouts  8.92 us (7%)
    pallas_call x1, Pallas kernels, per_device(): pl.pallas_call(kernel, out_shape=(jax.ShapeDtypeStruct((TOK, KB), BF16),...  123 us
    unnamed x9, local copies, waits for them, and re-layouts  7.03 us

profile of v1, /device:TPU:1, one launch (start us, length us, event | category | flops | bytes accessed | tf_op | source)
XLA Modules:
  0.0 132.3 jit_solution(13586608258659791879)
XLA Ops:
  0.6 1.4 %copy.14.routes_ref = s32[40,2]{1,0:T(8,128)} copy(s32[40,2]{0,1:T(2,128)} %param.8) | data formatting | bytes 640 | tf_op args[1]
  2.0 1.4 %copy.15.logits_ref = f32[40,2]{1,0:T(8,128)} copy(f32[40,2]{0,1:T(2,128)} %param.9) | data formatting | bytes 640 | tf_op args[2]
  3.4 122.8 %expert_handover.1 = (bf16[40,512]{1,0:T(8,128)(2,1)}, bf16[4096,128]{1,0:T(8,128)(2,1)}, bf16[4096,128]{1,0:T(8,128)(2,1)}, bf16[8,4,128,128]{3,2,1,0:T(8,128)(2,1)}) custom-call(bf16[40,4096]{1,0:T(8,128)(2,1)} %tok_hbm.1, s32[40,2]{1,0:T(8,128)} %copy.14.routes_ref, f32[40,2]{1,0:T(8,128)} %copy.15.logits_ref, f32[1,128]{1,0:T(1,128)} %bitcast.9, ...), custom_call_target="tpu_custom_call" | custom-call | tf_op jit(solution)/shard_map/expert_handover/pallas_call | solution.py:333
  126.1 0.0 copy-start.1
  126.1 1.0 reshape.17
  127.2 0.1 copy.16
  127.2 0.8 reshape.18
  128.0 0.0 copy-start
  128.0 2.4 %copy.20 = bf16[1,4096,128]{2,1,0:T(8,128)(2,1)} copy(bf16[1,4096,128]{2,1,0:T(8,128)(2,1)} %bitcast.7) | data formatting | bytes 2097152
  130.4 0.0 copy-done.1
  130.4 1.0 copy.21
  131.4 0.0 copy-done
  131.4 1.0 copy.22
Async XLA Ops:
  126.1 4.3 %copy-start.1 = (bf16[4096,128]{1,0:T(8,128)(2,1)S(1)}, bf16[4096,128]{1,0:T(8,128)(2,1)}, u32[]{:S(2)}) copy-start(bf16[4096,128]{1,0:T(8,128)(2,1)} %get-tuple-element.10) | copy-start | bytes 3145732
  128.0 3.3 %copy-start = (bf16[8,4,128,128]{3,2,1,0:T(8,128)(2,1)S(1)}, bf16[8,4,128,128]{3,2,1,0:T(8,128)(2,1)}, u32[]{:S(2)}) copy-start(bf16[8,4,128,128]{3,2,1,0:T(8,128)(2,1)} %get-tuple-element.11) | copy-start | bytes 3145732

commit v2 on v1

v2 whole, which is shorter than its diff:
```python
import functools

import jax
import jax.numpy as jnp
from jax import lax
from jax.experimental import pallas as pl
from jax.experimental.pallas import tpu as pltpu
from jax.sharding import PartitionSpec as P

MESH = pl.DeviceIdType.MESH
NZ, NX, NY = 8, 4, 4
NFS, NTP = 32, 8
EXPERTS = 4
D = 4096
KB = D // NTP
TOK = 40
SLOT = 32
ROWS = NFS * SLOT
XROWS = NZ * SLOT
NC = 4
DR = 128 // NC
CW = NX * DR
F32, BF16 = jnp.float32, jnp.bfloat16


def rem(a, n):
    return lax.rem(a, jnp.int32(n))


def div(a, n):
    return lax.div(a, jnp.int32(n))


def kernel(
    tok_hbm, routes_hbm, logits_hbm, gain_hbm, gate_hbm, up_hbm, down_hbm,
    mixed_ref, wgu, wd,
    tok, routes_ref, logits_ref, gain_ref, stage, wmix, p_send, sg, sd, xg, hid, dn, ro, r1, r2, rr,
    tok_sem, load_sem,
    t1_s, t1_r, t2_s, t2_r, t3_s, t3_r, t3f_s, cc_s, cc_r,
    gu_s, gu_r, wd_s, wd_r, h_s, h_r, hc_s, hc_r, dn_s, dn_r, r1_s, r1_r, r2_s, r2_r,
):
    fs, tp = lax.axis_index("fs"), lax.axis_index("tp")
    z, x = div(fs, NX), rem(fs, NX)
    y, core = div(tp, 2), rem(tp, 2)

    def rcopy(src, dst, ssem, rsem, fs2, tp2):
        return pltpu.make_async_remote_copy(
            src_ref=src, dst_ref=dst, send_sem=ssem, recv_sem=rsem,
            device_id=(fs2, tp2), device_id_type=MESH,
        )

    def wait_for(sem, ref):
        pltpu.make_async_copy(ref, ref, sem).wait()

    def tp_of(dy):
        return rem(y + dy, NY) * 2 + core

    other = y * 2 + (1 - core)

    small = [
        pltpu.make_async_copy(src, dst, tok_sem.at[i])
        for i, (src, dst) in enumerate(
            ((routes_hbm, routes_ref), (logits_hbm, logits_ref), (tok_hbm, tok), (gain_hbm, gain_ref))
        )
    ]
    for cp in small:
        cp.start()
    loads = []
    for m, hbm in enumerate((gate_hbm, up_hbm, down_hbm)):
        cp = pltpu.make_async_copy(hbm, stage.at[m], load_sem.at[m])
        cp.start()
        loads.append(cp)

    bar = pltpu.get_barrier_semaphore()

    @pl.loop(1, NFS)
    def _(i):
        pl.semaphore_signal(bar, inc=1, device_id=(rem(fs + i, NFS), tp), device_id_type=MESH)

    @pl.loop(1, NTP)
    def _(i):
        pl.semaphore_signal(bar, inc=1, device_id=(fs, rem(tp + i, NTP)), device_id_type=MESH)

    small[0].wait()
    small[1].wait()
    row = lax.broadcasted_iota(jnp.int32, (EXPERTS * SLOT, TOK), 0)
    row_e = div(row, SLOT)
    row_s = rem(row, SLOT).astype(F32)
    pick0 = jnp.where(routes_ref[0:1, :] == row_e, 1.0, 0.0).astype(F32)
    pick1 = jnp.where(routes_ref[1:2, :] == row_e, 1.0, 0.0).astype(F32)
    member = pick0 + pick1
    row_i = lax.broadcasted_iota(jnp.int32, (TOK, TOK), 0)
    col_i = lax.broadcasted_iota(jnp.int32, (TOK, TOK), 1)
    before = jnp.where(row_i < col_i, 1.0, 0.0).astype(BF16)
    position = jnp.dot(member.astype(BF16), before, preferred_element_type=F32)
    placing = jnp.where((position == row_s) & (member > 0.0), 1.0, 0.0).astype(F32)
    diff = logits_ref[0:1, :] - logits_ref[1:2, :]
    share0 = 1.0 / (1.0 + jnp.exp(-diff))
    share1 = 1.0 / (1.0 + jnp.exp(diff))
    wmix[...] = placing * (pick0 * share0 + pick1 * share1)

    small[2].wait()
    tf = tok[...].astype(F32)
    inv = lax.rsqrt(jnp.mean(tf * tf, axis=1, keepdims=True) + 1e-05)
    block = tok[:, pl.ds(pl.multiple_of(tp * KB, KB), KB)].astype(F32)
    normed = (block * inv).astype(BF16)
    packed = jnp.dot(placing.astype(BF16), normed, preferred_element_type=F32)
    p_send[...] = packed.astype(BF16).reshape(EXPERTS, SLOT, KB)
    own_x = pl.multiple_of(x * XROWS, XROWS)
    own_row = pl.multiple_of(x * XROWS + z * SLOT, SLOT)
    xg[tp, pl.ds(own_row, SLOT), :] = p_send[div(z, 2)]

    pl.semaphore_wait(bar, NFS - 1 + NTP - 1)

    for dz in (4, 3, 5, 2, 6, 1, 7):
        z2 = rem(z + dz, NZ)
        rcopy(
            p_send.at[div(z2, 2)], xg.at[tp, pl.ds(own_row, SLOT), :], t1_s, t1_r.at[dz],
            z2 * NX + x, tp,
        ).start()

    my_rows = pl.ds(pl.multiple_of(fs * 128, 128), 128)

    def send_gu(dz, dx):
        f2 = rem(z + dz, NZ) * NX + rem(x + dx, NX)
        rcopy(sg.at[f2], wgu.at[my_rows, :], gu_s, gu_r, f2, tp).start()

    def send_down(k, i):
        dx, dz = div(i, NZ), rem(i, NZ)
        f2 = rem(z + dz, NZ) * NX + rem(x + dx, NX)
        part = pl.ds(k * DR, DR)
        rcopy(
            sd.at[f2, part, :], wd.at[z, x, part, :], wd_s.at[k], wd_r.at[k], f2, tp
        ).start()

    small[3].wait()
    gain = jnp.transpose(jnp.broadcast_to(gain_ref[...], (128, 128)))
    for m in range(2):
        loads[m].wait()

        @pl.loop(0, EXPERTS)
        def _(e):
            for s in range(8):
                sg[e * 8 + s, :, m * 128 : (m + 1) * 128] = (
                    stage[m, e, :, s * 128 : (s + 1) * 128] * gain
                ).astype(BF16)

    wgu[pl.ds(pl.multiple_of(fs * 128, 128), 128), :] = sg[fs]

    @pl.loop(1, NZ)
    def _(dz):
        send_gu(dz, 0)

    loads[2].wait()

    @pl.loop(0, EXPERTS)
    def _(e):
        for s in range(8):
            sd[e * 8 + s] = stage[2, e, :, s * 128 : (s + 1) * 128].astype(BF16)

    wd[z, x] = sd[fs]

    def along_x(dz):
        piece = xg.at[tp, pl.ds(own_x + rem(z + NZ - dz, NZ) * SLOT, SLOT), :]
        if dz:
            wait_for(t1_r.at[dz], piece)
        for dx in (1, 3, 2):
            rcopy(
                piece, piece, t2_s, t2_r.at[dx - 1], z * NX + rem(x + dx, NX), tp
            ).start()

    for dz in (0, 1, 7, 2, 6, 3, 5, 4):
        along_x(dz)

    def part_of(t, p, half=None):
        base = rem(x + NX - p, NX) * XROWS
        if half is None:
            return xg.at[t, pl.ds(pl.multiple_of(base, XROWS), XROWS), :]
        h = XROWS // 2
        return xg.at[t, pl.ds(pl.multiple_of(base + half * h, h), h), :]

    def to_core(t, p):
        ref = part_of(t, p)
        rcopy(ref, ref, cc_s, cc_r, fs, other).start()

    def own_part(p):
        ref = part_of(tp, p)
        rcopy(ref, ref, t3_s, t3_r.at[0, p], fs, tp_of(1)).start()
        rcopy(ref, ref, t3_s, t3_r.at[1, p], fs, tp_of(3)).start()
        to_core(tp, p)

    own_part(0)

    def send_gu_from(dx):
        @pl.loop(0, NZ)
        def _(dz):
            send_gu(dz, dx)

    for p in range(1, NX):
        wait_for(t2_r.at[p - 1], part_of(tp, p))
        own_part(p)
        send_gu_from(p)
    for k in range(NC):

        @pl.loop(1, NFS)
        def _(i):
            send_down(k, i)

    for p in range(NX):
        below, above = tp_of(3), tp_of(1)
        ref = part_of(below, p)
        wait_for(t3_r.at[0, p], ref)
        half = part_of(below, p, 0)
        rcopy(half, half, t3f_s, t3_r.at[2, p], fs, above).start()
        to_core(below, p)
        ref = part_of(above, p)
        wait_for(t3_r.at[1, p], ref)
        half = part_of(above, p, 1)
        rcopy(half, half, t3f_s, t3_r.at[2, p], fs, below).start()
        to_core(above, p)
    for p in range(NX):
        wait_for(t3_r.at[2, p], part_of(tp_of(2), p))
        to_core(tp_of(2), p)
    wait_for(cc_r, xg.at[0:NY])
    wait_for(gu_r, wgu.at[0 : (NFS - 1) * 128, :])


    @pl.loop(0, NX)
    def _(r):
        rows = pl.ds(pl.multiple_of(r * XROWS, XROWS), XROWS)
        acc = jnp.zeros((XROWS, 256), F32)
        for t in range(NTP):
            acc += jnp.dot(
                xg[t, rows, :], wgu[t * KB : (t + 1) * KB, :], preferred_element_type=F32
            )
        g, u = acc[:, 0:128], acc[:, 128:256]
        hid[tp, rows, :] = (g / (1.0 + jnp.exp(-g)) * u).astype(BF16)

    def lanes_of(t):
        return hid.at[t]

    half = ROWS // 2

    def piece_of(t, h):
        return hid.at[t, h * half : (h + 1) * half, :]

    below, above = tp_of(3), tp_of(1)
    for h in (0, 1):
        up_piece, down_piece = piece_of(tp, h), piece_of(tp, 1 - h)
        rcopy(up_piece, up_piece, h_s, h_r.at[0, h], fs, above).start()
        rcopy(down_piece, down_piece, h_s, h_r.at[1, 1 - h], fs, below).start()
    own_h = lanes_of(tp)
    rcopy(own_h, own_h, hc_s, hc_r, fs, other).start()

    def h_core(t):
        rcopy(lanes_of(t), lanes_of(t), hc_s, hc_r, fs, other).start()

    def summed(k):
        wait_for(r1_r.at[k], r1.at[k])
        total = ro[k, x].astype(F32)
        for i in range(NX - 1):
            total += r1[k, i].astype(F32)
        r2[k] = total.astype(BF16).reshape(NZ, SLOT, CW)
        rr[k, z] = r2[k, z]

        @pl.loop(1, NZ)
        def _(dz):
            z2 = rem(z + dz, NZ)
            rcopy(
                r2.at[k, z2], rr.at[k, z], r2_s.at[k], r2_r.at[k], z2 * NX + x, tp
            ).start()

    def forward(k):
        part = slice(k * DR, (k + 1) * DR)
        wait_for(wd_r.at[k], sd.at[0 : NFS - 1, 0:DR, :])

        @pl.loop(1, NTP)
        def _(i):
            to = rem(tp + i, NTP)
            rcopy(
                wd.at[to, :, part, :], dn.at[k, tp], dn_s.at[k], dn_r.at[k], fs, to
            ).start()

        dn[k, tp] = wd[tp, :, part, :]

    def project(k):
        wait_for(dn_r.at[k], sd.at[0 : 4 * (NTP - 1), 0:DR, :])
        dnk = jnp.concatenate([dn[k, t].reshape(CW, 128) for t in range(NTP)], axis=1)
        for j in (1, 2, 3, 0):
            x2 = rem(x + j, NX)
            rows = pl.ds(pl.multiple_of(x2 * XROWS, XROWS), XROWS)
            ro[k, x2] = lax.dot_general(
                jnp.concatenate([hid[t, rows, :] for t in range(NTP)], axis=1),
                dnk, (((1,), (1,)), ((), ())), preferred_element_type=F32
            ).astype(BF16)
        for j in (1, 2, 3):
            x2 = rem(x + j, NX)
            rcopy(
                ro.at[k, x2], r1.at[k, j - 1], r1_s.at[k], r1_r.at[k], z * NX + x2, tp
            ).start()

    forward(0)
    wait_for(h_r.at[0, 0], piece_of(below, 0))
    rcopy(piece_of(below, 0), piece_of(below, 0), h_s, h_r.at[2, 0], fs, above).start()
    wait_for(h_r.at[1, 1], piece_of(above, 1))
    rcopy(piece_of(above, 1), piece_of(above, 1), h_s, h_r.at[2, 0], fs, below).start()
    wait_for(h_r.at[0, 1], piece_of(below, 1))
    h_core(below)
    wait_for(h_r.at[1, 0], piece_of(above, 0))
    h_core(above)
    forward(1)
    wait_for(h_r.at[2, 0], lanes_of(tp_of(2)))
    h_core(tp_of(2))
    forward(2)
    wait_for(hc_r, hid.at[0:NY])
    project(0)
    project(1)
    forward(3)
    project(2)
    summed(0)
    summed(1)
    project(3)
    summed(2)
    summed(3)

    for k in range(NC):
        wait_for(r2_r.at[k], r2.at[k, 0 : NZ - 1])
    per_expert = jnp.concatenate(
        [
            jnp.concatenate(
                [
                    rr[k, 2 * e].astype(F32) + rr[k, 2 * e + 1].astype(F32)
                    for e in range(EXPERTS)
                ],
                axis=0,
            )
            for k in range(NC)
        ],
        axis=1,
    )
    mixed = lax.dot_general(
        wmix[...], per_expert, (((0,), (0,)), ((), ())),
        precision=lax.Precision.HIGHEST, preferred_element_type=F32,
    )
    mixed_ref[...] = jnp.concatenate(
        [
            mixed[:, k * CW + i * DR : k * CW + (i + 1) * DR]
            for i in range(NX)
            for k in range(NC)
        ],
        axis=1,
    ).astype(BF16)

    wait_for(t1_s, xg.at[0, 0 : (NZ - 1) * SLOT, :])
    wait_for(t2_s, xg.at[0, 0 : (NX - 1) * XROWS, :])
    wait_for(t3_s, xg.at[0:2])
    wait_for(t3f_s, xg.at[0])
    wait_for(cc_s, xg.at[0:NY])
    wait_for(gu_s, wgu.at[0 : (NFS - 1) * 128, :])
    wait_for(h_s, hid.at[0 : NY - 1])
    wait_for(hc_s, hid.at[0:NY])
    for k in range(NC):
        wait_for(wd_s.at[k], sd.at[0 : NFS - 1, 0:DR, :])
        wait_for(dn_s.at[k], sd.at[0 : 4 * (NTP - 1), 0:DR, :])
        wait_for(r1_s.at[k], r1.at[k])
        wait_for(r2_s.at[k], r2.at[k, 0 : NZ - 1])


def write_out(mixed_ref, wgu, wd, gate_out, up_out, down_out, mixed_out, sem):
    copies = [
        pltpu.make_async_copy(wgu.at[:, 0:128], gate_out, sem.at[0]),
        pltpu.make_async_copy(wgu.at[:, 128:256], up_out, sem.at[1]),
        pltpu.make_async_copy(wd, down_out, sem.at[2]),
        pltpu.make_async_copy(mixed_ref, mixed_out, sem.at[3]),
    ]
    for cp in copies:
        cp.start()
    for cp in copies:
        cp.wait()


def per_device(tokens, routes, route_logits, norm_gain, gate_weight, up_weight, down_weight):
    dma = pltpu.SemaphoreType.DMA
    hbm = pl.BlockSpec(memory_space=pltpu.HBM)
    vmem = pl.BlockSpec(memory_space=pltpu.VMEM)
    mixed, wgu, wd = pl.pallas_call(
        kernel,
        out_shape=(
            pltpu.VMEM((TOK, KB), BF16),
            pltpu.VMEM((D, 256), BF16),
            pltpu.VMEM((NZ, NX, 128, 128), BF16),
        ),
        in_specs=[hbm] * 7,
        out_specs=(vmem, vmem, vmem),
        scratch_shapes=[
            pltpu.VMEM((TOK, D), BF16),
            pltpu.VMEM((2, TOK), jnp.int32),
            pltpu.VMEM((2, TOK), F32),
            pltpu.VMEM((1, 128), F32),
            pltpu.VMEM((3, EXPERTS, 128, 1024), F32),
            pltpu.VMEM((EXPERTS * SLOT, TOK), F32),
            pltpu.VMEM((EXPERTS, SLOT, KB), BF16),
            pltpu.VMEM((NFS, 128, 256), BF16),
            pltpu.VMEM((NFS, 128, 128), BF16),
            pltpu.VMEM((NTP, ROWS, KB), BF16),
            pltpu.VMEM((NTP, ROWS, 128), BF16),
            pltpu.VMEM((NC, NTP, NX, DR, 128), BF16),
            pltpu.VMEM((NC, NX, XROWS, CW), BF16),
            pltpu.VMEM((NC, NX - 1, XROWS, CW), BF16),
            pltpu.VMEM((NC, NZ, SLOT, CW), BF16),
            pltpu.VMEM((NC, NZ, SLOT, CW), BF16),
            dma((4,)), dma((3,)),
            dma, dma((NZ,)), dma, dma((NX - 1,)), dma, dma((3, NX)), dma, dma, dma,
            dma, dma, dma((NC,)), dma((NC,)), dma, dma((3, 2)), dma, dma,
            dma((NC,)), dma((NC,)), dma((NC,)), dma((NC,)), dma((NC,)), dma((NC,)),
        ],
        compiler_params=pltpu.CompilerParams(
            collective_id=0, has_side_effects=True, vmem_limit_bytes=48 * 2**20
        ),
        name="expert_handover",
    )(
        *(
            pltpu.with_memory_space_constraint(a, pltpu.HBM)
            for a in (
                tokens, routes.T, route_logits.T, norm_gain[None, :],
                gate_weight, up_weight, down_weight,
            )
        )
    )
    gate, up, down, mixed = pl.pallas_call(
        write_out,
        out_shape=(
            jax.ShapeDtypeStruct((D, 128), BF16),
            jax.ShapeDtypeStruct((D, 128), BF16),
            jax.ShapeDtypeStruct((NZ, NX, 128, 128), BF16),
            jax.ShapeDtypeStruct((TOK, KB), BF16),
        ),
        in_specs=[vmem, vmem, vmem],
        out_specs=(hbm, hbm, hbm, hbm),
        scratch_shapes=[dma((4,))],
        compiler_params=pltpu.CompilerParams(vmem_limit_bytes=2**20),
        name="write_out",
    )(*(pltpu.with_memory_space_constraint(a, pltpu.VMEM) for a in (mixed, wgu, wd)))
    return (mixed, gate[None], up[None], down.reshape(1, D, 128))


def solution(mesh):
    in_specs = (
        P("fs", None),
        P("fs", None),
        P("fs", None),
        P("fs"),
        P(None, "fs", "tp"),
        P(None, "fs", "tp"),
        P(None, "fs", "tp"),
    )
    out_specs = (P("fs", "tp"), P("tp", None, "fs"), P("tp", None, "fs"), P("tp", None, "fs"))
    return jax.shard_map(
        per_device, mesh=mesh, in_specs=in_specs, out_specs=out_specs, check_vma=False
    )
```

time: 133 us -> 113 us (0.85)
  Pallas kernels: 123 us -> 113 us
  local copies, waits for them, and re-layouts: 8.92 us -> 0 us
    pallas_call x1 -> x2, Pallas kernels: 123 us -> 113 us  [the longest x1 111 us: per_device(): pl.pallas_call(kernel, out_shape=(pltpu.VMEM((TOK, KB), BF16), pltpu.VMEM...]
    unnamed x9 -> x0, local copies, waits for them, and re-layouts: 7.03 us -> none
    reshape x2 -> x0, local copies, waits for them, and re-layouts: 1.82 us -> none  [per_device(): mixed.reshape(TOK, NC, NX, DR).transpose(0, 2, 1, 3).reshape(TOK, KB)]
where the time goes in v2:
time: 113 us
  Pallas kernels  113 us (100%)
    pallas_call x1, Pallas kernels, per_device(): pl.pallas_call(kernel, out_shape=(pltpu.VMEM((TOK, KB), BF16), pltpu.VMEM...  111 us

profile of v2, /device:TPU:1, one launch (start us, length us, event | category | flops | bytes accessed | tf_op | source)
XLA Modules:
  0.0 113.3 jit_solution(4097712271654602181)
XLA Ops:
  0.6 111.0 %expert_handover.1 = (bf16[40,512]{1,0:T(8,128)(2,1)S(1)}, bf16[4096,256]{1,0:T(8,128)(2,1)S(1)}, bf16[8,4,128,128]{3,2,1,0:T(8,128)(2,1)S(1)}) custom-call(bf16[40,4096]{1,0:T(8,128)(2,1)} %tok_hbm.1, s32[2,40]{1,0:T(2,128)} %bitcast.6, f32[2,40]{1,0:T(2,128)} %bitcast.7, f32[1,128]{1,0:T(1,128)} %bitcast.8, f32[4,128,1024]{2,1,0:T(8,128)} %gate_hbm.1, ...), custom_call_target="tpu_custom_call" | custom-call | tf_op jit(solution)/shard_map/expert_handover/pallas_call | solution.py:386
  111.6 1.7 %write_out.1 = (bf16[4096,128]{1,0:T(8,128)(2,1)}, bf16[4096,128]{1,0:T(8,128)(2,1)}, bf16[8,4,128,128]{3,2,1,0:T(8,128)(2,1)}, bf16[40,512]{1,0:T(8,128)(2,1)}) custom-call(bf16[40,512]{1,0:T(8,128)(2,1)S(1)} %get-tuple-element.11.mixed_ref, bf16[4096,256]{1,0:T(8,128)(2,1)S(1)} %get-tuple-element.12.wgu, bf16[8,4,128,128]{3,2,1,0:T(8,128)(2,1)S(1)} %get-tuple-element.13.wd), custom_call_target="tpu_custom_call" | custom-call | tf_op jit(solution)/shard_map/write_out/pallas_call | solution.py:430

commit v3 on v2

--- a/solution.py
+++ b/solution.py
@@ -37,7 +37,7 @@
     tok, routes_ref, logits_ref, gain_ref, stage, wmix, p_send, sg, sd, xg, hid, dn, ro, r1, r2, rr,
     tok_sem, load_sem,
     t1_s, t1_r, t2_s, t2_r, t3_s, t3_r, t3f_s, cc_s, cc_r,
-    gu_s, gu_r, wd_s, wd_r, h_s, h_r, hc_s, hc_r, dn_s, dn_r, r1_s, r1_r, r2_s, r2_r,
+    go, gu_s, gu_r, wd_s, wd_r, h_s, h_r, hc_s, hc_r, dn_s, dn_r, r1_s, r1_r, r2_s, r2_r,
 ):
     fs, tp = lax.axis_index("fs"), lax.axis_index("tp")
     z, x = div(fs, NX), rem(fs, NX)
@@ -200,11 +200,16 @@
         wait_for(t2_r.at[p - 1], part_of(tp, p))
         own_part(p)
         send_gu_from(p)
-    for k in range(NC):
-
-        @pl.loop(1, NFS)
-        def _(i):
-            send_down(k, i)
+    def send_all_down():
+        for k in range(NC):
+
+            @pl.loop(1, NFS)
+            def _(i):
+                send_down(k, i)
+
+    @pl.when(core == 0)
+    def _():
+        send_all_down()
 
     for p in range(NX):
         below, above = tp_of(3), tp_of(1)
@@ -222,6 +227,12 @@
         wait_for(t3_r.at[2, p], part_of(tp_of(2), p))
         to_core(tp_of(2), p)
     wait_for(cc_r, xg.at[0:NY])
+
+    @pl.when(core == 0)
+    def _():
+        wait_for(gu_s, wgu.at[0 : (NFS - 1) * 128, :])
+        pl.semaphore_signal(go, inc=1, device_id=(fs, other), device_id_type=MESH)
+
     wait_for(gu_r, wgu.at[0 : (NFS - 1) * 128, :])
 
 
@@ -299,18 +310,40 @@
                 ro.at[k, x2], r1.at[k, j - 1], r1_s.at[k], r1_r.at[k], z * NX + x2, tp
             ).start()
 
-    forward(0)
-    wait_for(h_r.at[0, 0], piece_of(below, 0))
-    rcopy(piece_of(below, 0), piece_of(below, 0), h_s, h_r.at[2, 0], fs, above).start()
-    wait_for(h_r.at[1, 1], piece_of(above, 1))
-    rcopy(piece_of(above, 1), piece_of(above, 1), h_s, h_r.at[2, 0], fs, below).start()
-    wait_for(h_r.at[0, 1], piece_of(below, 1))
-    h_core(below)
-    wait_for(h_r.at[1, 0], piece_of(above, 0))
-    h_core(above)
-    forward(1)
-    wait_for(h_r.at[2, 0], lanes_of(tp_of(2)))
-    h_core(tp_of(2))
+    @pl.when(core == 1)
+    def _():
+        pl.semaphore_wait(go, 1)
+        send_all_down()
+        wait_for(gu_s, wgu.at[0 : (NFS - 1) * 128, :])
+
+    def relay_near():
+        wait_for(h_r.at[0, 0], piece_of(below, 0))
+        rcopy(piece_of(below, 0), piece_of(below, 0), h_s, h_r.at[2, 0], fs, above).start()
+        wait_for(h_r.at[1, 1], piece_of(above, 1))
+        rcopy(piece_of(above, 1), piece_of(above, 1), h_s, h_r.at[2, 0], fs, below).start()
+        wait_for(h_r.at[0, 1], piece_of(below, 1))
+        h_core(below)
+        wait_for(h_r.at[1, 0], piece_of(above, 0))
+        h_core(above)
+
+    def relay_far():
+        wait_for(h_r.at[2, 0], lanes_of(tp_of(2)))
+        h_core(tp_of(2))
+
+    @pl.when(core == 0)
+    def _():
+        forward(0)
+        relay_near()
+        forward(1)
+        relay_far()
+
+    @pl.when(core == 1)
+    def _():
+        relay_near()
+        relay_far()
+        forward(0)
+        forward(1)
+
     forward(2)
     wait_for(hc_r, hid.at[0:NY])
     project(0)
@@ -356,7 +389,6 @@
     wait_for(t3_s, xg.at[0:2])
     wait_for(t3f_s, xg.at[0])
     wait_for(cc_s, xg.at[0:NY])
-    wait_for(gu_s, wgu.at[0 : (NFS - 1) * 128, :])
     wait_for(h_s, hid.at[0 : NY - 1])
     wait_for(hc_s, hid.at[0:NY])
     for k in range(NC):
@@ -411,6 +443,7 @@
             pltpu.VMEM((NC, NZ, SLOT, CW), BF16),
             dma((4,)), dma((3,)),
             dma, dma((NZ,)), dma, dma((NX - 1,)), dma, dma((3, NX)), dma, dma, dma,
+            pltpu.SemaphoreType.REGULAR,
             dma, dma, dma((NC,)), dma((NC,)), dma, dma((3, 2)), dma, dma,
             dma((NC,)), dma((NC,)), dma((NC,)), dma((NC,)), dma((NC,)), dma((NC,)),
         ],

time: 113 us -> 109 us (0.965)
  Pallas kernels: 113 us -> 109 us
    pallas_call x1, Pallas kernels: 111 us -> 107 us  [per_device(): pl.pallas_call(kernel, out_shape=(pltpu.VMEM((TOK, KB), BF16), pltpu.VMEM...]
where the time goes in v3:
time: 109 us
  Pallas kernels  109 us (100%)
    pallas_call x1, Pallas kernels, per_device(): pl.pallas_call(kernel, out_shape=(pltpu.VMEM((TOK, KB), BF16), pltpu.VMEM...  107 us

profile of v3, /device:TPU:1, one launch (start us, length us, event | category | flops | bytes accessed | tf_op | source)
XLA Modules:
  0.0 109.2 jit_solution(383581968909050882)
XLA Ops:
  0.6 106.8 %expert_handover.1 = (bf16[40,512]{1,0:T(8,128)(2,1)S(1)}, bf16[4096,256]{1,0:T(8,128)(2,1)S(1)}, bf16[8,4,128,128]{3,2,1,0:T(8,128)(2,1)S(1)}) custom-call(bf16[40,4096]{1,0:T(8,128)(2,1)} %tok_hbm.1, s32[2,40]{1,0:T(2,128)} %bitcast.6, f32[2,40]{1,0:T(2,128)} %bitcast.7, f32[1,128]{1,0:T(1,128)} %bitcast.8, f32[4,128,1024]{2,1,0:T(8,128)} %gate_hbm.1, ...), custom_call_target="tpu_custom_call" | custom-call | tf_op jit(solution)/shard_map/expert_handover/pallas_call | solution.py:418
  107.5 1.7 %write_out.1 = (bf16[4096,128]{1,0:T(8,128)(2,1)}, bf16[4096,128]{1,0:T(8,128)(2,1)}, bf16[8,4,128,128]{3,2,1,0:T(8,128)(2,1)}, bf16[40,512]{1,0:T(8,128)(2,1)}) custom-call(bf16[40,512]{1,0:T(8,128)(2,1)S(1)} %get-tuple-element.11.mixed_ref, bf16[4096,256]{1,0:T(8,128)(2,1)S(1)} %get-tuple-element.12.wgu, bf16[8,4,128,128]{3,2,1,0:T(8,128)(2,1)S(1)} %get-tuple-element.13.wd), custom_call_target="tpu_custom_call" | custom-call | tf_op jit(solution)/shard_map/write_out/pallas_call | solution.py:463

commit v4 on v3

--- a/solution.py
+++ b/solution.py
@@ -17,8 +17,9 @@
 SLOT = 32
 ROWS = NFS * SLOT
 XROWS = NZ * SLOT
-NC = 4
-DR = 128 // NC
+CHUNKS = ((0, 32), (32, 32), (64, 32), (96, 16), (112, 16))
+NC = len(CHUNKS)
+DR = 32
 CW = NX * DR
 F32, BF16 = jnp.float32, jnp.bfloat16
 
@@ -31,10 +32,14 @@
     return lax.div(a, jnp.int32(n))
 
 
+def slots_of(k):
+    return SLOT * CHUNKS[k][1] // DR
+
+
 def kernel(
     tok_hbm, routes_hbm, logits_hbm, gain_hbm, gate_hbm, up_hbm, down_hbm,
-    mixed_ref, wgu, wd,
-    tok, routes_ref, logits_ref, gain_ref, stage, wmix, p_send, sg, sd, xg, hid, dn, ro, r1, r2, rr,
+    wmix, rr, wgu, wd,
+    tok, routes_ref, logits_ref, gain_ref, stage, p_send, sg, sd, xg, hid, dn, ro, r1, r2,
     tok_sem, load_sem,
     t1_s, t1_r, t2_s, t2_r, t3_s, t3_r, t3f_s, cc_s, cc_r,
     go, gu_s, gu_r, wd_s, wd_r, h_s, h_r, hc_s, hc_r, dn_s, dn_r, r1_s, r1_r, r2_s, r2_r,
@@ -128,7 +133,7 @@
     def send_down(k, i):
         dx, dz = div(i, NZ), rem(i, NZ)
         f2 = rem(z + dz, NZ) * NX + rem(x + dx, NX)
-        part = pl.ds(k * DR, DR)
+        part = pl.ds(*CHUNKS[k])
         rcopy(
             sd.at[f2, part, :], wd.at[z, x, part, :], wd_s.at[k], wd_r.at[k], f2, tp
         ).start()
@@ -267,47 +272,57 @@
         rcopy(lanes_of(t), lanes_of(t), hc_s, hc_r, fs, other).start()
 
     def summed(k):
-        wait_for(r1_r.at[k], r1.at[k])
-        total = ro[k, x].astype(F32)
+        n = slots_of(k)
+        wait_for(r1_r.at[k], r1.at[k, :, 0 : NZ * n])
+        total = ro[k, x, 0 : NZ * n].astype(F32)
         for i in range(NX - 1):
-            total += r1[k, i].astype(F32)
-        r2[k] = total.astype(BF16).reshape(NZ, SLOT, CW)
-        rr[k, z] = r2[k, z]
+            total += r1[k, i, 0 : NZ * n].astype(F32)
+        r2[k, :, 0:n] = total.astype(BF16).reshape(NZ, n, CW)
+        rr[k, z, 0:n] = r2[k, z, 0:n]
 
         @pl.loop(1, NZ)
         def _(dz):
             z2 = rem(z + dz, NZ)
             rcopy(
-                r2.at[k, z2], rr.at[k, z], r2_s.at[k], r2_r.at[k], z2 * NX + x, tp
+                r2.at[k, z2, 0:n], rr.at[k, z, 0:n], r2_s.at[k], r2_r.at[k], z2 * NX + x, tp
             ).start()
 
     def forward(k):
-        part = slice(k * DR, (k + 1) * DR)
-        wait_for(wd_r.at[k], sd.at[0 : NFS - 1, 0:DR, :])
+        start, size = CHUNKS[k]
+        part = slice(start, start + size)
+        wait_for(wd_r.at[k], sd.at[0 : NFS - 1, 0:size, :])
 
         @pl.loop(1, NTP)
         def _(i):
             to = rem(tp + i, NTP)
             rcopy(
-                wd.at[to, :, part, :], dn.at[k, tp], dn_s.at[k], dn_r.at[k], fs, to
+                wd.at[to, :, part, :], dn.at[k, tp, :, 0:size, :], dn_s.at[k], dn_r.at[k], fs, to
             ).start()
 
-        dn[k, tp] = wd[tp, :, part, :]
+        dn[k, tp, :, 0:size, :] = wd[tp, :, part, :]
 
     def project(k):
-        wait_for(dn_r.at[k], sd.at[0 : 4 * (NTP - 1), 0:DR, :])
-        dnk = jnp.concatenate([dn[k, t].reshape(CW, 128) for t in range(NTP)], axis=1)
+        size, n = CHUNKS[k][1], slots_of(k)
+        wait_for(dn_r.at[k], sd.at[0 : 4 * (NTP - 1), 0:size, :])
+        dnk = jnp.concatenate(
+            [dn[k, t, :, 0:size, :].reshape(NX * size, 128) for t in range(NTP)], axis=1
+        )
         for j in (1, 2, 3, 0):
             x2 = rem(x + j, NX)
             rows = pl.ds(pl.multiple_of(x2 * XROWS, XROWS), XROWS)
-            ro[k, x2] = lax.dot_general(
+            out = lax.dot_general(
                 jnp.concatenate([hid[t, rows, :] for t in range(NTP)], axis=1),
-                dnk, (((1,), (1,)), ((), ())), preferred_element_type=F32
-            ).astype(BF16)
+                dnk, (((1,), (1,)), ((), ())), preferred_element_type=F32,
+            )
+            if n < SLOT:
+                out = out.reshape(NZ, 2, n, NX * size)
+                out = jnp.concatenate([out[:, 0], out[:, 1]], axis=-1).reshape(NZ * n, CW)
+            ro[k, x2, 0 : NZ * n] = out.astype(BF16)
         for j in (1, 2, 3):
             x2 = rem(x + j, NX)
             rcopy(
-                ro.at[k, x2], r1.at[k, j - 1], r1_s.at[k], r1_r.at[k], z * NX + x2, tp
+                ro.at[k, x2, 0 : NZ * n], r1.at[k, j - 1, 0 : NZ * n], r1_s.at[k], r1_r.at[k],
+                z * NX + x2, tp,
             ).start()
 
     @pl.when(core == 1)
@@ -336,6 +351,7 @@
         relay_near()
         forward(1)
         relay_far()
+        forward(2)
 
     @pl.when(core == 1)
     def _():
@@ -344,29 +360,63 @@
         forward(0)
         forward(1)
 
-    forward(2)
     wait_for(hc_r, hid.at[0:NY])
     project(0)
+
+    @pl.when(core == 1)
+    def _():
+        forward(2)
+
+    forward(3)
     project(1)
-    forward(3)
+    forward(4)
+    summed(0)
     project(2)
-    summed(0)
     summed(1)
     project(3)
+    project(4)
     summed(2)
     summed(3)
+    summed(4)
 
     for k in range(NC):
-        wait_for(r2_r.at[k], r2.at[k, 0 : NZ - 1])
+        wait_for(r2_r.at[k], r2.at[k, 0 : NZ - 1, 0 : slots_of(k)])
+
+    wait_for(t1_s, xg.at[0, 0 : (NZ - 1) * SLOT, :])
+    wait_for(t2_s, xg.at[0, 0 : (NX - 1) * XROWS, :])
+    wait_for(t3_s, xg.at[0:2])
+    wait_for(t3f_s, xg.at[0])
+    wait_for(cc_s, xg.at[0:NY])
+    wait_for(h_s, hid.at[0 : NY - 1])
+    wait_for(hc_s, hid.at[0:NY])
+    for k in range(NC):
+        size, n = CHUNKS[k][1], slots_of(k)
+        wait_for(wd_s.at[k], sd.at[0 : NFS - 1, 0:size, :])
+        wait_for(dn_s.at[k], sd.at[0 : 4 * (NTP - 1), 0:size, :])
+        wait_for(r1_s.at[k], r1.at[k, :, 0 : NZ * n])
+        wait_for(r2_s.at[k], r2.at[k, 0 : NZ - 1, 0:n])
+
+
+def write_out(wmix, rr, wgu, wd, gate_out, up_out, down_out, mixed_out, mixed_ref, sem):
+    copies = [
+        pltpu.make_async_copy(wgu.at[:, 0:128], gate_out, sem.at[0]),
+        pltpu.make_async_copy(wgu.at[:, 128:256], up_out, sem.at[1]),
+        pltpu.make_async_copy(wd, down_out, sem.at[2]),
+        pltpu.make_async_copy(mixed_ref, mixed_out, sem.at[3]),
+    ]
+    for cp in copies[:3]:
+        cp.start()
+
+    def returned(k, e):
+        n = slots_of(k)
+        both = rr[k, 2 * e, 0:n].astype(F32) + rr[k, 2 * e + 1, 0:n].astype(F32)
+        if n == SLOT:
+            return both
+        return jnp.concatenate([both[:, : CW // 2], both[:, CW // 2 :]], axis=0)
+
     per_expert = jnp.concatenate(
         [
-            jnp.concatenate(
-                [
-                    rr[k, 2 * e].astype(F32) + rr[k, 2 * e + 1].astype(F32)
-                    for e in range(EXPERTS)
-                ],
-                axis=0,
-            )
+            jnp.concatenate([returned(k, e) for e in range(EXPERTS)], axis=0)
             for k in range(NC)
         ],
         axis=1,
@@ -377,36 +427,13 @@
     )
     mixed_ref[...] = jnp.concatenate(
         [
-            mixed[:, k * CW + i * DR : k * CW + (i + 1) * DR]
+            mixed[:, NX * start + i * size : NX * start + (i + 1) * size]
             for i in range(NX)
-            for k in range(NC)
+            for start, size in CHUNKS
         ],
         axis=1,
     ).astype(BF16)
-
-    wait_for(t1_s, xg.at[0, 0 : (NZ - 1) * SLOT, :])
-    wait_for(t2_s, xg.at[0, 0 : (NX - 1) * XROWS, :])
-    wait_for(t3_s, xg.at[0:2])
-    wait_for(t3f_s, xg.at[0])
-    wait_for(cc_s, xg.at[0:NY])
-    wait_for(h_s, hid.at[0 : NY - 1])
-    wait_for(hc_s, hid.at[0:NY])
-    for k in range(NC):
-        wait_for(wd_s.at[k], sd.at[0 : NFS - 1, 0:DR, :])
-        wait_for(dn_s.at[k], sd.at[0 : 4 * (NTP - 1), 0:DR, :])
-        wait_for(r1_s.at[k], r1.at[k])
-        wait_for(r2_s.at[k], r2.at[k, 0 : NZ - 1])
-
-
-def write_out(mixed_ref, wgu, wd, gate_out, up_out, down_out, mixed_out, sem):
-    copies = [
-        pltpu.make_async_copy(wgu.at[:, 0:128], gate_out, sem.at[0]),
-        pltpu.make_async_copy(wgu.at[:, 128:256], up_out, sem.at[1]),
-        pltpu.make_async_copy(wd, down_out, sem.at[2]),
-        pltpu.make_async_copy(mixed_ref, mixed_out, sem.at[3]),
-    ]
-    for cp in copies:
-        cp.start()
+    copies[3].start()
     for cp in copies:
         cp.wait()
 
@@ -415,22 +442,22 @@
     dma = pltpu.SemaphoreType.DMA
     hbm = pl.BlockSpec(memory_space=pltpu.HBM)
     vmem = pl.BlockSpec(memory_space=pltpu.VMEM)
-    mixed, wgu, wd = pl.pallas_call(
+    held = pl.pallas_call(
         kernel,
         out_shape=(
-            pltpu.VMEM((TOK, KB), BF16),
+            pltpu.VMEM((EXPERTS * SLOT, TOK), F32),
+            pltpu.VMEM((NC, NZ, SLOT, CW), BF16),
             pltpu.VMEM((D, 256), BF16),
             pltpu.VMEM((NZ, NX, 128, 128), BF16),
         ),
         in_specs=[hbm] * 7,
-        out_specs=(vmem, vmem, vmem),
+        out_specs=(vmem,) * 4,
         scratch_shapes=[
             pltpu.VMEM((TOK, D), BF16),
             pltpu.VMEM((2, TOK), jnp.int32),
             pltpu.VMEM((2, TOK), F32),
             pltpu.VMEM((1, 128), F32),
             pltpu.VMEM((3, EXPERTS, 128, 1024), F32),
-            pltpu.VMEM((EXPERTS * SLOT, TOK), F32),
             pltpu.VMEM((EXPERTS, SLOT, KB), BF16),
             pltpu.VMEM((NFS, 128, 256), BF16),
             pltpu.VMEM((NFS, 128, 128), BF16),
@@ -439,7 +466,6 @@
             pltpu.VMEM((NC, NTP, NX, DR, 128), BF16),
             pltpu.VMEM((NC, NX, XROWS, CW), BF16),
             pltpu.VMEM((NC, NX - 1, XROWS, CW), BF16),
-            pltpu.VMEM((NC, NZ, SLOT, CW), BF16),
             pltpu.VMEM((NC, NZ, SLOT, CW), BF16),
             dma((4,)), dma((3,)),
             dma, dma((NZ,)), dma, dma((NX - 1,)), dma, dma((3, NX)), dma, dma, dma,
@@ -468,12 +494,12 @@
             jax.ShapeDtypeStruct((NZ, NX, 128, 128), BF16),
             jax.ShapeDtypeStruct((TOK, KB), BF16),
         ),
-        in_specs=[vmem, vmem, vmem],
+        in_specs=[vmem] * 4,
         out_specs=(hbm, hbm, hbm, hbm),
-        scratch_shapes=[dma((4,))],
-        compiler_params=pltpu.CompilerParams(vmem_limit_bytes=2**20),
+        scratch_shapes=[pltpu.VMEM((TOK, KB), BF16), dma((4,))],
+        compiler_params=pltpu.CompilerParams(vmem_limit_bytes=6 * 2**20),
         name="write_out",
-    )(*(pltpu.with_memory_space_constraint(a, pltpu.VMEM) for a in (mixed, wgu, wd)))
+    )(*(pltpu.with_memory_space_constraint(a, pltpu.VMEM) for a in held))
     return (mixed, gate[None], up[None], down.reshape(1, D, 128))
 
 

time: 109 us -> 107 us (0.982)
  Pallas kernels: 109 us -> 106 us
    pallas_call x1, Pallas kernels: 107 us -> 105 us  [per_device(): pl.pallas_call(kernel, out_shape=(pltpu.VMEM((EXPERTS * SLOT, TOK), F32),...]
where the time goes in v4:
time: 107 us
  Pallas kernels  106 us (99%)
    pallas_call x1, Pallas kernels, per_device(): pl.pallas_call(kernel, out_shape=(pltpu.VMEM((EXPERTS * SLOT, TOK), F32),...  105 us

profile of v4, /device:TPU:1, one launch (start us, length us, event | category | flops | bytes accessed | tf_op | source)
XLA Modules:
  0.0 107.0 jit_solution(13229887496156868166)
XLA Ops:
  0.6 104.7 %expert_handover.1 = (f32[128,40]{1,0:T(8,128)S(1)}, bf16[5,8,32,128]{3,2,1,0:T(8,128)(2,1)S(1)}, bf16[4096,256]{1,0:T(8,128)(2,1)S(1)}, bf16[8,4,128,128]{3,2,1,0:T(8,128)(2,1)S(1)}) custom-call(bf16[40,4096]{1,0:T(8,128)(2,1)} %tok_hbm.1, s32[2,40]{1,0:T(2,128)} %bitcast.6, f32[2,40]{1,0:T(2,128)} %bitcast.7, f32[1,128]{1,0:T(1,128)} %bitcast.8, ...), custom_call_target="tpu_custom_call" | custom-call | tf_op jit(solution)/shard_map/expert_handover/pallas_call | solution.py:445
  105.3 1.7 %write_out.1 = (bf16[4096,128]{1,0:T(8,128)(2,1)}, bf16[4096,128]{1,0:T(8,128)(2,1)}, bf16[8,4,128,128]{3,2,1,0:T(8,128)(2,1)}, bf16[40,512]{1,0:T(8,128)(2,1)}) custom-call(f32[128,40]{1,0:T(8,128)S(1)} %get-tuple-element.12.wmix, bf16[5,8,32,128]{3,2,1,0:T(8,128)(2,1)S(1)} %get-tuple-element.13.rr, bf16[4096,256]{1,0:T(8,128)(2,1)S(1)} %get-tuple-element.14.wgu, ...), custom_call_target="tpu_custom_call" | custom-call | tf_op jit(solution)/shard_map/write_out/pallas_call | solution.py:489

commit v5 on v4

--- a/solution.py
+++ b/solution.py
@@ -17,7 +17,7 @@
 SLOT = 32
 ROWS = NFS * SLOT
 XROWS = NZ * SLOT
-CHUNKS = ((0, 32), (32, 32), (64, 32), (96, 16), (112, 16))
+CHUNKS = ((0, 32), (32, 32), (64, 16), (80, 16), (96, 16), (112, 16))
 NC = len(CHUNKS)
 DR = 32
 CW = NX * DR
@@ -205,8 +205,8 @@
         wait_for(t2_r.at[p - 1], part_of(tp, p))
         own_part(p)
         send_gu_from(p)
-    def send_all_down():
-        for k in range(NC):
+    def send_chunks(first, end):
+        for k in range(first, end):
 
             @pl.loop(1, NFS)
             def _(i):
@@ -214,7 +214,7 @@
 
     @pl.when(core == 0)
     def _():
-        send_all_down()
+        send_chunks(0, NC)
 
     for p in range(NX):
         below, above = tp_of(3), tp_of(1)
@@ -239,6 +239,10 @@
         pl.semaphore_signal(go, inc=1, device_id=(fs, other), device_id_type=MESH)
 
     wait_for(gu_r, wgu.at[0 : (NFS - 1) * 128, :])
+
+    @pl.when(core == 1)
+    def _():
+        send_chunks(0, 1)
 
 
     @pl.loop(0, NX)
@@ -328,7 +332,7 @@
     @pl.when(core == 1)
     def _():
         pl.semaphore_wait(go, 1)
-        send_all_down()
+        send_chunks(1, NC)
         wait_for(gu_s, wgu.at[0 : (NFS - 1) * 128, :])
 
     def relay_near():
@@ -370,14 +374,17 @@
     forward(3)
     project(1)
     forward(4)
+    project(2)
     summed(0)
-    project(2)
+    forward(5)
+    project(3)
     summed(1)
-    project(3)
     project(4)
     summed(2)
+    project(5)
     summed(3)
     summed(4)
+    summed(5)
 
     for k in range(NC):
         wait_for(r2_r.at[k], r2.at[k, 0 : NZ - 1, 0 : slots_of(k)])

time: 107 us -> 107 us (level)
  no operation moved by 1% of the time
where the time goes in v5:
time: 107 us
  Pallas kernels  106 us (99%)
    pallas_call x1, Pallas kernels, per_device(): pl.pallas_call(kernel, out_shape=(pltpu.VMEM((EXPERTS * SLOT, TOK), F32),...  104 us

profile of v5, /device:TPU:1, one launch (start us, length us, event | category | flops | bytes accessed | tf_op | source)
XLA Modules:
  0.0 106.7 jit_solution(3811562937353861388)
XLA Ops:
  0.6 104.4 %expert_handover.1 = (f32[128,40]{1,0:T(8,128)S(1)}, bf16[6,8,32,128]{3,2,1,0:T(8,128)(2,1)S(1)}, bf16[4096,256]{1,0:T(8,128)(2,1)S(1)}, bf16[8,4,128,128]{3,2,1,0:T(8,128)(2,1)S(1)}) custom-call(bf16[40,4096]{1,0:T(8,128)(2,1)} %tok_hbm.1, s32[2,40]{1,0:T(2,128)} %bitcast.6, f32[2,40]{1,0:T(2,128)} %bitcast.7, f32[1,128]{1,0:T(1,128)} %bitcast.8, ...), custom_call_target="tpu_custom_call" | custom-call | tf_op jit(solution)/shard_map/expert_handover/pallas_call | solution.py:452
  105.0 1.7 %write_out.1 = (bf16[4096,128]{1,0:T(8,128)(2,1)}, bf16[4096,128]{1,0:T(8,128)(2,1)}, bf16[8,4,128,128]{3,2,1,0:T(8,128)(2,1)}, bf16[40,512]{1,0:T(8,128)(2,1)}) custom-call(f32[128,40]{1,0:T(8,128)S(1)} %get-tuple-element.12.wmix, bf16[6,8,32,128]{3,2,1,0:T(8,128)(2,1)S(1)} %get-tuple-element.13.rr, bf16[4096,256]{1,0:T(8,128)(2,1)S(1)} %get-tuple-element.14.wgu, ...), custom_call_target="tpu_custom_call" | custom-call | tf_op jit(solution)/shard_map/write_out/pallas_call | solution.py:496

commit v6 on v5

--- a/solution.py
+++ b/solution.py
@@ -378,10 +378,10 @@
     summed(0)
     forward(5)
     project(3)
+    project(4)
     summed(1)
-    project(4)
+    project(5)
     summed(2)
-    project(5)
     summed(3)
     summed(4)
     summed(5)

time: 107 us -> 106 us (level)
  no operation moved by 1% of the time
where the time goes in v6:
time: 106 us
  Pallas kernels  106 us (100%)
    pallas_call x1, Pallas kernels, per_device(): pl.pallas_call(kernel, out_shape=(pltpu.VMEM((EXPERTS * SLOT, TOK), F32),...  104 us

profile of v6, /device:TPU:1, one launch (start us, length us, event | category | flops | bytes accessed | tf_op | source)
XLA Modules:
  0.0 106.4 jit_solution(17030577159355501768)
XLA Ops:
  0.6 104.1 %expert_handover.1 = (f32[128,40]{1,0:T(8,128)S(1)}, bf16[6,8,32,128]{3,2,1,0:T(8,128)(2,1)S(1)}, bf16[4096,256]{1,0:T(8,128)(2,1)S(1)}, bf16[8,4,128,128]{3,2,1,0:T(8,128)(2,1)S(1)}) custom-call(bf16[40,4096]{1,0:T(8,128)(2,1)} %tok_hbm.1, s32[2,40]{1,0:T(2,128)} %bitcast.6, f32[2,40]{1,0:T(2,128)} %bitcast.7, f32[1,128]{1,0:T(1,128)} %bitcast.8, ...), custom_call_target="tpu_custom_call" | custom-call | tf_op jit(solution)/shard_map/expert_handover/pallas_call | solution.py:452
  104.7 1.7 %write_out.1 = (bf16[4096,128]{1,0:T(8,128)(2,1)}, bf16[4096,128]{1,0:T(8,128)(2,1)}, bf16[8,4,128,128]{3,2,1,0:T(8,128)(2,1)}, bf16[40,512]{1,0:T(8,128)(2,1)}) custom-call(f32[128,40]{1,0:T(8,128)S(1)} %get-tuple-element.12.wmix, bf16[6,8,32,128]{3,2,1,0:T(8,128)(2,1)S(1)} %get-tuple-element.13.rr, bf16[4096,256]{1,0:T(8,128)(2,1)S(1)} %get-tuple-element.14.wgu, ...), custom_call_target="tpu_custom_call" | custom-call | tf_op jit(solution)/shard_map/write_out/pallas_call | solution.py:496
